TPU v7x, 32 devices: a whole 2x2x4 slice. The times are simulated.
32 devices in a mesh: kv: 8 (over z, y), tp: 4 (over x, core).
Axes of the slice: x: 2, y: 2, z: 4, core: 2. Of those that a mesh axis runs over, the one named last changes fastest.
Arguments:
- tokens: bfloat16 [16, 3072], P('kv', 'tp'), may hold values from -15 to 15
- associative_state: float32 [16, 16, 128, 128], P('kv', 'tp'), may hold values from -2 to 2
- sudden_extra_decay: float32 [16, 16], P('kv', 'tp'), may hold values from -0.7 to 0
- head_decay_speed: float32 [16], P('tp'), may hold values from 0.05 to 2
- opening_norm_gain: float32 [3072], P('tp'), may hold values from 0.1 to 1.9
- opening_gate_weight: bfloat16 [3072, 8448], P('tp', 'kv'), may hold values from -0.109375 to 0.109375
- opening_up_weight: bfloat16 [3072, 8448], P('tp', 'kv'), may hold values from -0.109375 to 0.109375
- opening_down_weight: bfloat16 [8448, 3072], P('kv', 'tp'), may hold values from -0.25 to 0.25
- mixer_norm_gain: float32 [3072], P('tp'), may hold values from 0.1 to 1.9
- query_matrix: bfloat16 [3072, 2048], P('tp'), may hold values from -0.109375 to 0.109375
- key_matrix: bfloat16 [3072, 2048], P('tp'), may hold values from -0.109375 to 0.109375
- value_matrix: bfloat16 [3072, 2048], P('tp'), may hold values from -0.109375 to 0.109375
- output_gate_matrix: bfloat16 [3072, 2048], P('tp'), may hold values from -0.109375 to 0.109375
- strength_weight: bfloat16 [3072, 16], P('tp'), may hold values from -0.109375 to 0.109375
- decay_matrix: bfloat16 [3072, 16], P('tp'), may hold values from -0.109375 to 0.109375
- head_read_gain: float32 [128], replicated, may hold values from 0.1 to 1.9
- output_matrix: bfloat16 [2048, 3072], P('tp'), may hold values from -0.125 to 0.125
- closing_norm_gain: float32 [3072], P('tp'), may hold values from 0.1 to 1.9
- closing_gate_weight: bfloat16 [3072, 8448], P('tp', 'kv'), may hold values from -0.109375 to 0.109375
- closing_up_weight: bfloat16 [3072, 8448], P('tp', 'kv'), may hold values from -0.109375 to 0.109375
- closing_down_weight: bfloat16 [8448, 3072], P('kv', 'tp'), may hold values from -0.25 to 0.25
Outputs:
- layer_out: bfloat16 [16, 3072], P('kv', 'tp')
- memory_new: float32 [16, 16, 128, 128], P('kv', 'tp')
All inputs are finite; a program needn't handle non-finite values.
Results may differ from a plain program's by a relative error of at most 0.023.
Values may be sent and summed in bfloat16 or wider, within the bound.
A program may use at most 64 MiB of HBM per device.

v0:
```python
import jax
import jax.numpy as jnp
from jax import lax
from jax.sharding import PartitionSpec as P

norm_eps = 1e-06


def feed_forward(resid, rows_in, gain, gate_proj, lift_proj, down_proj):
    model_width = gain.shape[0] * lax.axis_size("tp")
    gathered = lax.all_gather(rows_in, "kv", axis=0, tiled=True)
    values = gathered.astype(jnp.float32)
    scaled = (values * gain).astype(jnp.bfloat16)
    gate_part = jnp.dot(scaled, gate_proj, preferred_element_type=jnp.float32)
    lift_part = jnp.dot(scaled, lift_proj, preferred_element_type=jnp.float32)
    square = jnp.sum(values * values, axis=1)
    gate_sum, lift_sum, square_sum = (
        lax.psum(gate_part.astype(jnp.bfloat16), "tp").astype(jnp.float32),
        lax.psum(lift_part.astype(jnp.bfloat16), "tp").astype(jnp.float32),
        lax.psum(square.astype(jnp.bfloat16), "tp").astype(jnp.float32),
    )
    scale_of_norm = lax.rsqrt(square_sum / model_width + norm_eps)[:, None]
    hidden = (jax.nn.silu(scale_of_norm * gate_sum) * (scale_of_norm * lift_sum)).astype(
        jnp.bfloat16
    )
    down_part = jnp.dot(hidden, down_proj, preferred_element_type=jnp.float32)
    whole_sum = lax.psum(down_part, "kv")
    row_count = resid.shape[0]
    own_rows = lax.dynamic_slice_in_dim(whole_sum, lax.axis_index("kv") * row_count, row_count, 0)
    return resid + 0.5 * own_rows.astype(jnp.bfloat16).astype(jnp.float32)


def unit_norm(values):
    return values * lax.rsqrt(jnp.sum(values * values, axis=-1, keepdims=True) + 1e-12)


def body(
    tokens,
    associative_state,
    sudden_extra_decay,
    head_decay_speed,
    opening_norm_gain,
    opening_gate_weight,
    opening_up_weight,
    opening_down_weight,
    mixer_norm_gain,
    query_matrix,
    key_matrix,
    value_matrix,
    output_gate_matrix,
    strength_weight,
    decay_matrix,
    head_read_gain,
    output_matrix,
    closing_norm_gain,
    closing_gate_weight,
    closing_up_weight,
    closing_down_weight,
):
    model_width = opening_norm_gain.shape[0] * lax.axis_size("tp")
    first = feed_forward(
        tokens.astype(jnp.float32),
        tokens,
        opening_norm_gain,
        opening_gate_weight,
        opening_up_weight,
        opening_down_weight,
    )
    square_sum = lax.psum(jnp.sum(first * first, axis=1), "tp")
    scale_of_norm = lax.rsqrt(square_sum / model_width + norm_eps)[:, None]
    mixer_input = (first * mixer_norm_gain).astype(jnp.bfloat16)
    partials = tuple(
        (
            jnp.dot(mixer_input, weight, preferred_element_type=jnp.float32).astype(jnp.bfloat16)
            for weight in (
                query_matrix,
                key_matrix,
                value_matrix,
                output_gate_matrix,
                strength_weight,
                decay_matrix,
            )
        )
    )
    query_sum, key_sum, value_sum, gate_sum, beta_sum, decay_total = (
        lax.psum_scatter(partials[0], "tp", scatter_dimension=1, tiled=True).astype(jnp.float32),
        lax.psum_scatter(partials[1], "tp", scatter_dimension=1, tiled=True).astype(jnp.float32),
        lax.psum_scatter(partials[2], "tp", scatter_dimension=1, tiled=True).astype(jnp.float32),
        lax.psum_scatter(partials[3], "tp", scatter_dimension=1, tiled=True).astype(jnp.float32),
        lax.psum_scatter(partials[4], "tp", scatter_dimension=1, tiled=True).astype(jnp.float32),
        lax.psum_scatter(partials[5], "tp", scatter_dimension=1, tiled=True).astype(jnp.float32),
    )
    row_count = query_sum.shape[0]
    head_count = head_decay_speed.shape[0]
    head_size = head_read_gain.shape[0]

    def split_heads(values):
        return (scale_of_norm * values).reshape(row_count, head_count, head_size)

    query_vec = unit_norm(split_heads(query_sum)) * head_size ** (-0.5)
    key_vec = unit_norm(split_heads(key_sum))
    value_vec = split_heads(value_sum)
    gate_vec = split_heads(gate_sum)
    beta = jax.nn.sigmoid(scale_of_norm * beta_sum)
    decay_logarithm = (
        -head_decay_speed * jax.nn.softplus(scale_of_norm * decay_total) + sudden_extra_decay
    )
    kept = jnp.exp(decay_logarithm)[:, :, None, None]
    recall = jnp.einsum(
        "bhk,bhkv->bhv", key_vec, associative_state, precision=lax.Precision.HIGHEST
    )
    written = (beta[:, :, None] * key_vec)[:, :, :, None]
    memory_new = (
        kept * (associative_state - written * recall[:, :, None, :])
        + written * value_vec[:, :, None, :]
    )
    read_out = jnp.einsum("bhk,bhkv->bhv", query_vec, memory_new, precision=lax.Precision.HIGHEST)
    normed = read_out * lax.rsqrt(jnp.mean(read_out * read_out, axis=-1, keepdims=True) + norm_eps)
    normed = normed * head_read_gain * jax.nn.silu(gate_vec)
    mix_out = normed.reshape(row_count, head_count * head_size).astype(jnp.bfloat16)
    out_part = jnp.dot(mix_out, output_matrix, preferred_element_type=jnp.float32).astype(
        jnp.bfloat16
    )
    mixed = lax.psum_scatter(out_part, "tp", scatter_dimension=1, tiled=True).astype(jnp.float32)
    second = first + mixed.astype(jnp.bfloat16).astype(jnp.float32)
    final = feed_forward(
        second,
        second.astype(jnp.bfloat16),
        closing_norm_gain,
        closing_gate_weight,
        closing_up_weight,
        closing_down_weight,
    )
    return (final.astype(jnp.bfloat16), memory_new)


def solution(mesh):
    placed = (
        P("kv", "tp"),
        P("kv", "tp", None, None),
        P("kv", "tp"),
        P("tp"),
        P("tp"),
        P("tp", "kv"),
        P("tp", "kv"),
        P("kv", "tp"),
        P("tp"),
        P("tp", None),
        P("tp", None),
        P("tp", None),
        P("tp", None),
        P("tp", None),
        P("tp", None),
        P(),
        P("tp", None),
        P("tp"),
        P("tp", "kv"),
        P("tp", "kv"),
        P("kv", "tp"),
    )
    return jax.shard_map(
        body,
        mesh=mesh,
        in_specs=placed,
        out_specs=(P("kv", "tp"), P("kv", "tp", None, None)),
        check_vma=False,
    )
```

profile of v0, /device:TPU:0, one launch (start us, length us, event | category | flops | bytes accessed | tf_op | source)
XLA Modules:
  0.0 359.4 jit_solution(2355526956701864364)
XLA Ops:
  7.2 32.6 %all-gather = bf16[8,2,768]{2,1,0:T(2,128)(2,1)S(1)} all-gather(bf16[1,2,768]{2,1,0:T(2,128)(2,1)} %bitcast.66), channel_id=1, replica_groups=mesh['kv'=8,'tp'=4] {'kv'}, dimensions={0}, use_global_device_ids=true | all-gather | bytes 27648 | tf_op jit(solution)/shard_map/all_gather | solution.py:11
  40.5 2.6 convolution_convert_fusion.3
  43.2 1.2 convolution_convert_fusion.4
  45.7 29.5 %all-reduce.10.cloned.1.call-done = (bf16[16,1056]{1,0:T(8,128)(2,1)}, bf16[16,1056]{1,0:T(8,128)(2,1)}, bf16[16]{0:T(256)(128)(2,1)}) async-done(((bf16[16,1056]{1,0:T(8,128)(2,1)}, bf16[16,1056]{1,0:T(8,128)(2,1)}, bf16[16]{0:T(256)(128)(2,1)}), (bf16[16,1056]{1,0:T(8,128)(2,1)}, bf16[16,1056]{1,0:T(8,128)(2,1)}, bf16[16]{0:T(256)(128)(2,1)})) %all-reduce.10.cloned.1.call-update) | async-done | bytes 67632 | tf_op jit(solution)/shard_map/psum | solution.py:19
  75.9 1.9 fusion
  77.7 37.9 %psum.66 = bf16[16,768]{1,0:T(8,128)(2,1)S(1)} all-reduce(f32[16,768]{1,0:T(8,128)S(1)} %fusion), channel_id=1, replica_groups=mesh['kv'=8,'tp'=4] {'kv'}, use_global_device_ids=true, to_apply=%region_4.5 | all-reduce | flops 12288 | bytes 73728 | tf_op jit(solution)/shard_map/psum | solution.py:27
  115.8 2.6 convolution_convert_fusion.5
  119.0 1.4 copy-done.2
  122.1 2.4 convolution_convert_fusion.7
  127.0 5.6 %psum.67 = f32[2]{0:T(128)S(1)} all-reduce(f32[2]{0:T(128)S(1)} %get-tuple-element.12), channel_id=1, replica_groups=mesh['kv'=8,'tp'=4] {'tp'}, use_global_device_ids=true, to_apply=%region_6.7 | all-reduce | flops 2 | bytes 16 | tf_op jit(solution)/shard_map/psum | solution.py:69
  133.8 7.8 %all-reduce.3 = (bf16[2,16]{1,0:T(2,128)(2,1)S(1)}, bf16[2,16]{1,0:T(2,128)(2,1)S(1)}) all-reduce(bf16[2,16]{1,0:T(2,128)(2,1)S(1)} %convolution_convert_fusion.9, bf16[2,16]{1,0:T(2,128)(2,1)S(1)} %convolution_convert_fusion.10), channel_id=4, replica_groups=mesh['kv'=8,'tp'=4] {'tp'}, use_global_device_ids=true, to_apply=%region_10.11.clone | all-reduce | flops 64 | bytes 256
  142.7 23.7 %reduce-scatter.20.cloned.1.call-done = bf16[512,2]{1,0:T(8,128)(2,1)} async-done(((bf16[2048,2]{1,0:T(8,128)(2,1)}), bf16[512,2]{1,0:T(8,128)(2,1)}) %reduce-scatter.20.cloned.1.call-update) | async-done | bytes 2064
  167.4 23.0 %reduce-scatter.22.cloned.1.call-done = bf16[512,2]{1,0:T(8,128)(2,1)} async-done(((bf16[2048,2]{1,0:T(8,128)(2,1)}), bf16[512,2]{1,0:T(8,128)(2,1)}) %reduce-scatter.22.cloned.1.call-update) | async-done | bytes 2064
  191.4 23.0 %reduce-scatter.24.cloned.1.call-done = bf16[512,2]{1,0:T(8,128)(2,1)} async-done(((bf16[2048,2]{1,0:T(8,128)(2,1)}), bf16[512,2]{1,0:T(8,128)(2,1)}) %reduce-scatter.24.cloned.1.call-update) | async-done | bytes 2064
  216.0 1.6 fusion.18
  217.6 1.3 multiply_add_fusion
  220.9 1.2 copy.37
  222.2 23.3 %reduce-scatter.26.cloned.1.call-done = bf16[768,2]{1,0:T(8,128)(2,1)} async-done(((bf16[3072,2]{1,0:T(8,128)(2,1)}), bf16[768,2]{1,0:T(8,128)(2,1)}) %reduce-scatter.26.cloned.1.call-update) | async-done | bytes 3088
  246.6 30.6 %all-gather.1 = bf16[8,2,768]{2,1,0:T(2,128)(2,1)S(1)} all-gather(bf16[1,2,768]{2,1,0:T(2,128)(2,1)S(1)} %fusion.9), channel_id=1, replica_groups=mesh['kv'=8,'tp'=4] {'kv'}, dimensions={0}, use_global_device_ids=true | all-gather | bytes 27648 | tf_op jit(solution)/shard_map/all_gather | solution.py:11
  277.9 2.6 convolution_convert_fusion.1
  280.4 1.2 convolution_convert_fusion.2
  281.6 29.9 %all-reduce.8.cloned.1.call-done = (bf16[16,1056]{1,0:T(8,128)(2,1)}, bf16[16,1056]{1,0:T(8,128)(2,1)}, bf16[16]{0:T(256)(128)(2,1)}) async-done(((bf16[16,1056]{1,0:T(8,128)(2,1)}, bf16[16,1056]{1,0:T(8,128)(2,1)}, bf16[16]{0:T(256)(128)(2,1)}), (bf16[16,1056]{1,0:T(8,128)(2,1)}, bf16[16,1056]{1,0:T(8,128)(2,1)}, bf16[16]{0:T(256)(128)(2,1)})) %all-reduce.8.cloned.1.call-update) | async-done | bytes 67632 | tf_op jit(solution)/shard_map/psum | solution.py:19
  312.2 1.9 fusion.1
  314.1 37.9 %psum.71 = bf16[16,768]{1,0:T(8,128)(2,1)S(1)} all-reduce(f32[16,768]{1,0:T(8,128)S(1)} %fusion.1), channel_id=1, replica_groups=mesh['kv'=8,'tp'=4] {'kv'}, use_global_device_ids=true, to_apply=%region_21.22 | all-reduce | flops 12288 | bytes 73728 | tf_op jit(solution)/shard_map/psum | solution.py:27
  (87 shorter events, 17.9 us)
Async XLA Ops:
  7.2 213.2 %copy-start = (bf16[512,3072]{1,0:T(8,128)(2,1)S(1)}, bf16[512,3072]{1,0:T(8,128)(2,1)}, u32[]{:S(2)}) copy-start(bf16[512,3072]{1,0:T(8,128)(2,1)} %param.37) | copy-start | bytes 9437188
  7.2 36.0 %copy-start.7 = (f32[768]{0:T(1024)S(1)}, f32[768]{0:T(1024)}, u32[]{:S(2)}) copy-start(f32[768]{0:T(1024)} %param.25) | copy-start | bytes 9220
  7.2 68.0 %all-reduce.10.cloned.1.call-start = ((), (), s32[]{:S(2)}) async-start(), calls=%async_computation.11 | async-start | bytes 148480 | tf_op jit(solution)/shard_map/psum | solution.py:19
  39.9 3.3 copy-start.4
  40.5 3.9 %copy-start.14 = (f32[4]{0:T(128)S(1)}, f32[4]{0:T(128)}, u32[]{:S(2)}) copy-start(f32[4]{0:T(128)} %param.24) | copy-start | bytes 52
  40.5 3.9 %copy-start.15 = (u32[32]{0:T(128)S(1)}, u32[32]{0:T(128)}, u32[]{:S(2)}) copy-start(u32[32]{0:T(128)} %constant.47) | copy-start | bytes 388
  43.1 72.5 %copy-start.6 = (bf16[2,768]{1,0:T(2,128)(2,1)S(1)}, bf16[2,768]{1,0:T(2,128)(2,1)}, u32[]{:S(2)}) copy-start(bf16[2,768]{1,0:T(2,128)(2,1)} %param.21) | copy-start | bytes 9220
  43.1 72.5 %copy-start.9 = (f32[768]{0:T(1024)S(1)}, f32[768]{0:T(1024)}, u32[]{:S(2)}) copy-start(f32[768]{0:T(1024)} %param.29) | copy-start | bytes 9220
  44.3 97.4 %reduce-scatter.18.cloned.1.call-start = ((), (), s32[]{:S(2)}) async-start(), calls=%async_computation.5 | async-start | bytes 655360
  115.7 2.8 copy-start.1
  118.5 1.9 copy-start.2
  122.0 3.6 %copy-start.12 = (bf16[768,16]{0,1:T(8,128)(2,1)S(1)}, bf16[768,16]{0,1:T(8,128)(2,1)}, u32[]{:S(2)}) copy-start(bf16[768,16]{0,1:T(8,128)(2,1)} %param.34) | copy-start | bytes 73732
  122.0 44.3 %reduce-scatter.20.cloned.1.call-start = ((), (), s32[]{:S(2)}) async-start(), calls=%async_computation.6 | async-start | bytes 655360
  124.5 2.4 copy-start.13
  125.6 90.3 %copy-start.10 = (f32[2,4]{1,0:T(2,128)S(1)}, f32[2,4]{1,0:T(2,128)}, u32[]{:S(2)}) copy-start(f32[2,4]{1,0:T(2,128)} %param.23) | copy-start | bytes 100
  125.6 64.8 %reduce-scatter.22.cloned.1.call-start = ((), (), s32[]{:S(2)}) async-start(), calls=%async_computation.7 | async-start | bytes 655360
  126.8 87.6 %reduce-scatter.24.cloned.1.call-start = ((), (), s32[]{:S(2)}) async-start(), calls=%async_computation.8 | async-start | bytes 655360
  133.7 86.6 %copy-start.11 = (f32[128]{0:T(128)S(1)}, f32[128]{0:T(128)}, u32[]{:S(2)}) copy-start(f32[128]{0:T(128)} %param.36) | copy-start | bytes 1540
  133.8 111.8 %reduce-scatter.26.cloned.1.call-start = ((), (), s32[]{:S(2)}) async-start(), calls=%async_computation.9 | async-start | bytes 983040
  218.9 0.8 copy-start.3
  220.9 57.0 %copy-start.8 = (f32[768]{0:T(1024)S(1)}, f32[768]{0:T(1024)}, u32[]{:S(2)}) copy-start(f32[768]{0:T(1024)} %param.38) | copy-start | bytes 9220
  222.2 89.4 %all-reduce.8.cloned.1.call-start = ((), (), s32[]{:S(2)}) async-start(), calls=%async_computation.10 | async-start | bytes 148480 | tf_op jit(solution)/shard_map/psum | solution.py:19
  277.2 3.2 copy-start.5
Sparse Core Ops, SparseCore 0:
  44.5 30.7 all-reduce.9
  122.1 19.5 reduce-scatter.17
  144.8 21.5 reduce-scatter.19
  168.7 21.6 reduce-scatter.21
  192.7 21.6 reduce-scatter.23
  222.3 23.2 reduce-scatter.25
  281.7 29.7 all-reduce.7
where the time goes:
time: 360 us; the launch traced here: 359 us
  waiting for transfers between devices  153 us (42%)
  blocking collectives  152 us (42%)
  matrix products  20.1 us (6%)
  between operations  15 us (4%)
  local copies, waits for them, and re-layouts  13.6 us (4%)
  other arithmetic  5.3 us (1%)
    unnamed x12, waiting for transfers between devices  93.2 us
    psum x2, blocking collectives, feed_forward(): whole_sum = lax.psum(down_part, 'kv')  75.8 us
    all_gather x2, blocking collectives, feed_forward(): gathered = lax.all_gather(rows_in, 'kv', axis=0, tiled=True)  63.2 us
    psum x2, waiting for transfers between devices, feed_forward(): lax.psum(lift_part.astype(jnp.bfloat16), 'tp').astype(jnp.float32)  59.4 us
    unnamed x43, local copies, waits for them, and re-layouts  13.5 us
    unnamed x1, blocking collectives  7.82 us
  transfers between devices with their start and end apart: 7, of which 7 were waited for; matrix products, arithmetic and copies ran while one was open for 3% of the time, Pallas kernels for 0%

commit v1 on v0

--- a/solution.py
+++ b/solution.py
@@ -8,7 +8,13 @@
 
 def feed_forward(resid, rows_in, gain, gate_proj, lift_proj, down_proj):
     model_width = gain.shape[0] * lax.axis_size("tp")
-    gathered = lax.all_gather(rows_in, "kv", axis=0, tiled=True)
+
+    def _lead_paths(shard_in):
+        last = jnp.stack([shard_in for _ in range(jax.lax.axis_size("kv"))])
+        clean = jax.lax.all_to_all(last, axis_name="kv", split_axis=0, concat_axis=0)
+        return jnp.concatenate(clean, axis=0)
+
+    gathered = _lead_paths(rows_in)
     values = gathered.astype(jnp.float32)
     scaled = (values * gain).astype(jnp.bfloat16)
     gate_part = jnp.dot(scaled, gate_proj, preferred_element_type=jnp.float32)

time: 360 us -> 317 us (0.88)
  blocking collectives: 152 us -> 115 us
  waiting for transfers between devices: 153 us -> 146 us
    all_gather x2 -> x0, blocking collectives: 63.2 us -> none  [feed_forward(): gathered = lax.all_gather(rows_in, 'kv', axis=0, tiled=True)]
    all_to_all x0 -> x2, blocking collectives: none -> 25.8 us  [_lead_paths(): jax.lax.all_to_all(last, axis_name='kv', split_axis=0, concat_axis=0)]
    psum x2, waiting for transfers between devices: 59.4 us -> 52.5 us  [feed_forward(): lax.psum(lift_part.astype(jnp.bfloat16), 'tp').astype(jnp.float32)]
where the time goes in v1:
time: 317 us; the launch traced here: 316 us
  waiting for transfers between devices  146 us (46%)
  blocking collectives  115 us (36%)
  matrix products  20.3 us (6%)
  local copies, waits for them, and re-layouts  15.7 us (5%)
  between operations  15 us (5%)
  other arithmetic  4.27 us (1%)
    unnamed x12, waiting for transfers between devices  93.2 us
    psum x2, blocking collectives, feed_forward(): whole_sum = lax.psum(down_part, 'kv')  75.8 us
    psum x2, waiting for transfers between devices, feed_forward(): lax.psum(lift_part.astype(jnp.bfloat16), 'tp').astype(jnp.float32)  52.5 us
    all_to_all x2, blocking collectives, _lead_paths(): jax.lax.all_to_all(last, axis_name='kv', split_axis=0, concat_axis=0)  25.8 us
    unnamed x43, local copies, waits for them, and re-layouts  13.5 us
    unnamed x1, blocking collectives  7.82 us
  transfers between devices with their start and end apart: 7, of which 7 were waited for; matrix products, arithmetic and copies ran while one was open for 3% of the time, Pallas kernels for 0%

profile of v1, /device:TPU:0, one launch (start us, length us, event | category | flops | bytes accessed | tf_op | source)
XLA Modules:
  0.0 316.4 jit_solution(3337487044434063234)
XLA Ops:
  8.1 13.9 %all_to_all.10 = bf16[8,2,768]{2,1,0:T(2,128)(2,1)S(1)} all-to-all(bf16[8,2,768]{2,1,0:T(2,128)(2,1)S(1)} %stack.4), channel_id=1, replica_groups=mesh['kv'=8,'tp'=4] {'kv'}, dimensions={0} | all-to-all | bytes 49152 | tf_op jit(solution)/shard_map/all_to_all | solution.py:14
  22.7 2.7 convolution_convert_fusion.3
  25.5 1.2 convolution_convert_fusion.4
  28.0 26.0 %all-reduce.10.cloned.1.call-done = (bf16[16,1056]{1,0:T(8,128)(2,1)}, bf16[16,1056]{1,0:T(8,128)(2,1)}, bf16[16]{0:T(256)(128)(2,1)}) async-done(((bf16[16,1056]{1,0:T(8,128)(2,1)}, bf16[16,1056]{1,0:T(8,128)(2,1)}, bf16[16]{0:T(256)(128)(2,1)}), (bf16[16,1056]{1,0:T(8,128)(2,1)}, bf16[16,1056]{1,0:T(8,128)(2,1)}, bf16[16]{0:T(256)(128)(2,1)})) %all-reduce.10.cloned.1.call-update) | async-done | bytes 67632 | tf_op jit(solution)/shard_map/psum | solution.py:25
  54.7 1.9 fusion
  56.6 37.9 %psum.66 = bf16[16,768]{1,0:T(8,128)(2,1)S(1)} all-reduce(f32[16,768]{1,0:T(8,128)S(1)} %fusion), channel_id=1, replica_groups=mesh['kv'=8,'tp'=4] {'kv'}, use_global_device_ids=true, to_apply=%region_4.5 | all-reduce | flops 12288 | bytes 73728 | tf_op jit(solution)/shard_map/psum | solution.py:33
  94.7 2.6 convolution_convert_fusion.5
  97.9 1.4 copy-done.2
  100.9 2.4 convolution_convert_fusion.7
  105.9 5.6 %psum.67 = f32[2]{0:T(128)S(1)} all-reduce(f32[2]{0:T(128)S(1)} %get-tuple-element.12), channel_id=1, replica_groups=mesh['kv'=8,'tp'=4] {'tp'}, use_global_device_ids=true, to_apply=%region_6.7 | all-reduce | flops 2 | bytes 16 | tf_op jit(solution)/shard_map/psum | solution.py:75
  112.7 7.8 %all-reduce.3 = (bf16[2,16]{1,0:T(2,128)(2,1)S(1)}, bf16[2,16]{1,0:T(2,128)(2,1)S(1)}) all-reduce(bf16[2,16]{1,0:T(2,128)(2,1)S(1)} %convolution_convert_fusion.9, bf16[2,16]{1,0:T(2,128)(2,1)S(1)} %convolution_convert_fusion.10), channel_id=4, replica_groups=mesh['kv'=8,'tp'=4] {'tp'}, use_global_device_ids=true, to_apply=%region_10.11.clone | all-reduce | flops 64 | bytes 256
  121.5 23.7 %reduce-scatter.20.cloned.1.call-done = bf16[512,2]{1,0:T(8,128)(2,1)} async-done(((bf16[2048,2]{1,0:T(8,128)(2,1)}), bf16[512,2]{1,0:T(8,128)(2,1)}) %reduce-scatter.20.cloned.1.call-update) | async-done | bytes 2064
  146.2 23.0 %reduce-scatter.22.cloned.1.call-done = bf16[512,2]{1,0:T(8,128)(2,1)} async-done(((bf16[2048,2]{1,0:T(8,128)(2,1)}), bf16[512,2]{1,0:T(8,128)(2,1)}) %reduce-scatter.22.cloned.1.call-update) | async-done | bytes 2064
  170.3 23.0 %reduce-scatter.24.cloned.1.call-done = bf16[512,2]{1,0:T(8,128)(2,1)} async-done(((bf16[2048,2]{1,0:T(8,128)(2,1)}), bf16[512,2]{1,0:T(8,128)(2,1)}) %reduce-scatter.24.cloned.1.call-update) | async-done | bytes 2064
  194.9 1.6 fusion.17
  196.4 1.3 multiply_add_fusion
  199.7 1.2 copy.43
  201.0 23.3 %reduce-scatter.26.cloned.1.call-done = bf16[768,2]{1,0:T(8,128)(2,1)} async-done(((bf16[3072,2]{1,0:T(8,128)(2,1)}), bf16[768,2]{1,0:T(8,128)(2,1)}) %reduce-scatter.26.cloned.1.call-update) | async-done | bytes 3088
  225.4 11.9 %all_to_all.11 = bf16[8,2,768]{2,1,0:T(2,128)(2,1)S(1)} all-to-all(bf16[8,2,768]{2,1,0:T(2,128)(2,1)S(1)} %stack.5), channel_id=1, replica_groups=mesh['kv'=8,'tp'=4] {'kv'}, dimensions={0} | all-to-all | bytes 49152 | tf_op jit(solution)/shard_map/all_to_all | solution.py:14
  238.1 2.7 convolution_convert_fusion.1
  240.9 1.2 convolution_convert_fusion.2
  242.0 26.5 %all-reduce.8.cloned.1.call-done = (bf16[16,1056]{1,0:T(8,128)(2,1)}, bf16[16,1056]{1,0:T(8,128)(2,1)}, bf16[16]{0:T(256)(128)(2,1)}) async-done(((bf16[16,1056]{1,0:T(8,128)(2,1)}, bf16[16,1056]{1,0:T(8,128)(2,1)}, bf16[16]{0:T(256)(128)(2,1)}), (bf16[16,1056]{1,0:T(8,128)(2,1)}, bf16[16,1056]{1,0:T(8,128)(2,1)}, bf16[16]{0:T(256)(128)(2,1)})) %all-reduce.8.cloned.1.call-update) | async-done | bytes 67632 | tf_op jit(solution)/shard_map/psum | solution.py:25
  269.2 1.9 fusion.1
  271.0 37.9 %psum.71 = bf16[16,768]{1,0:T(8,128)(2,1)S(1)} all-reduce(f32[16,768]{1,0:T(8,128)S(1)} %fusion.1), channel_id=1, replica_groups=mesh['kv'=8,'tp'=4] {'kv'}, use_global_device_ids=true, to_apply=%region_21.22 | all-reduce | flops 12288 | bytes 73728 | tf_op jit(solution)/shard_map/psum | solution.py:33
  (91 shorter events, 18.9 us)
Async XLA Ops:
  7.2 192.0 %copy-start = (bf16[512,3072]{1,0:T(8,128)(2,1)S(1)}, bf16[512,3072]{1,0:T(8,128)(2,1)}, u32[]{:S(2)}) copy-start(bf16[512,3072]{1,0:T(8,128)(2,1)} %param.37) | copy-start | bytes 9437188
  7.2 18.3 %copy-start.7 = (f32[768]{0:T(1024)S(1)}, f32[768]{0:T(1024)}, u32[]{:S(2)}) copy-start(f32[768]{0:T(1024)} %param.25) | copy-start | bytes 9220
  7.2 46.9 %all-reduce.10.cloned.1.call-start = ((), (), s32[]{:S(2)}) async-start(), calls=%async_computation.13 | async-start | bytes 148480 | tf_op jit(solution)/shard_map/psum | solution.py:25
  22.7 2.8 copy-start.4
  22.7 4.0 %copy-start.14 = (f32[4]{0:T(128)S(1)}, f32[4]{0:T(128)}, u32[]{:S(2)}) copy-start(f32[4]{0:T(128)} %param.24) | copy-start | bytes 52
  22.7 4.0 %copy-start.15 = (u32[32]{0:T(128)S(1)}, u32[32]{0:T(128)}, u32[]{:S(2)}) copy-start(u32[32]{0:T(128)} %constant.47) | copy-start | bytes 388
  25.5 69.0 %copy-start.6 = (bf16[2,768]{1,0:T(2,128)(2,1)S(1)}, bf16[2,768]{1,0:T(2,128)(2,1)}, u32[]{:S(2)}) copy-start(bf16[2,768]{1,0:T(2,128)(2,1)} %param.21) | copy-start | bytes 9220
  25.5 69.0 %copy-start.9 = (f32[768]{0:T(1024)S(1)}, f32[768]{0:T(1024)}, u32[]{:S(2)}) copy-start(f32[768]{0:T(1024)} %param.29) | copy-start | bytes 9220
  26.7 93.9 %reduce-scatter.18.cloned.1.call-start = ((), (), s32[]{:S(2)}) async-start(), calls=%async_computation.7 | async-start | bytes 655360
  94.5 2.8 copy-start.1
  97.3 1.9 copy-start.2
  100.9 3.6 %copy-start.12 = (bf16[768,16]{0,1:T(8,128)(2,1)S(1)}, bf16[768,16]{0,1:T(8,128)(2,1)}, u32[]{:S(2)}) copy-start(bf16[768,16]{0,1:T(8,128)(2,1)} %param.34) | copy-start | bytes 73732
  100.9 44.3 %reduce-scatter.20.cloned.1.call-start = ((), (), s32[]{:S(2)}) async-start(), calls=%async_computation.8 | async-start | bytes 655360
  103.3 2.4 copy-start.13
  104.4 90.3 %copy-start.10 = (f32[2,4]{1,0:T(2,128)S(1)}, f32[2,4]{1,0:T(2,128)}, u32[]{:S(2)}) copy-start(f32[2,4]{1,0:T(2,128)} %param.23) | copy-start | bytes 100
  104.4 64.8 %reduce-scatter.22.cloned.1.call-start = ((), (), s32[]{:S(2)}) async-start(), calls=%async_computation.9 | async-start | bytes 655360
  105.7 87.6 %reduce-scatter.24.cloned.1.call-start = ((), (), s32[]{:S(2)}) async-start(), calls=%async_computation.10 | async-start | bytes 655360
  112.6 86.6 %copy-start.11 = (f32[128]{0:T(128)S(1)}, f32[128]{0:T(128)}, u32[]{:S(2)}) copy-start(f32[128]{0:T(128)} %param.36) | copy-start | bytes 1540
  112.6 111.7 %reduce-scatter.26.cloned.1.call-start = ((), (), s32[]{:S(2)}) async-start(), calls=%async_computation.11 | async-start | bytes 983040
  197.7 0.8 copy-start.3
  199.7 38.4 %copy-start.8 = (f32[768]{0:T(1024)S(1)}, f32[768]{0:T(1024)}, u32[]{:S(2)}) copy-start(f32[768]{0:T(1024)} %param.38) | copy-start | bytes 9220
  201.0 67.5 %all-reduce.8.cloned.1.call-start = ((), (), s32[]{:S(2)}) async-start(), calls=%async_computation.12 | async-start | bytes 148480 | tf_op jit(solution)/shard_map/psum | solution.py:25
  238.1 2.7 copy-start.5
Sparse Core Ops, SparseCore 0:
  26.8 27.2 all-reduce.9
  101.0 19.5 reduce-scatter.17
  123.6 21.5 reduce-scatter.19
  147.6 21.6 reduce-scatter.21
  171.6 21.6 reduce-scatter.23
  201.1 23.1 reduce-scatter.25
  242.2 26.3 all-reduce.7
